TPU v7x, 512 devices: a whole 4x8x8 slice. The times are simulated.
512 devices in a mesh: kv: 64 (over z, y), tp: 8 (over x, core).
Axes of the slice: x: 4, y: 8, z: 8, core: 2. Of those that a mesh axis runs over, the one named last changes fastest.
Arguments:
- tokens: bfloat16 [1024, 2048], P('kv', 'tp'), may hold values from -20 to 20
- norm_gain: float32 [2048], replicated, may hold values from 0.1 to 1.9
- w_query: bfloat16 [2048, 1024], P(None, 'tp'), may hold values from -0.125 to 0.125
- w_key: bfloat16 [2048, 1024], P(None, 'tp'), may hold values from -0.125 to 0.125
- w_value: bfloat16 [2048, 1024], P(None, 'tp'), may hold values from -0.125 to 0.125
- w_outgate: bfloat16 [2048, 1024], P(None, 'tp'), may hold values from -0.125 to 0.125
- w_input_gate: bfloat16 [2048, 8], replicated, may hold values from -0.125 to 0.125
- w_forget_gate: bfloat16 [2048, 8], replicated, may hold values from -0.125 to 0.125
- memory: float32 [1024, 8, 128, 128], P('kv', 'tp'), may hold values from -6 to 6
- normalizer: float32 [1024, 8, 128], P('kv', 'tp'), may hold values from -6 to 6
- memory_max: float32 [1024, 8], P('kv', 'tp'), may hold values from -2 to 300
- w_output: bfloat16 [1024, 2048], P(None, 'tp'), may hold values from -0.1875 to 0.1875
- ffn_gain: float32 [2048], P('tp'), may hold values from 0.1 to 1.9
- w_gate: bfloat16 [2048, 5632], P('tp', 'kv'), may hold values from -0.125 to 0.125
- w_up: bfloat16 [2048, 5632], P('tp', 'kv'), may hold values from -0.125 to 0.125
- w_down: bfloat16 [5632, 2048], P('kv', 'tp'), may hold values from -0.078125 to 0.078125
Outputs:
- result: bfloat16 [1024, 2048], P('kv', 'tp')
- new_memory: float32 [1024, 8, 128, 128], P('kv', 'tp')
- new_normalizer: float32 [1024, 8, 128], P('kv', 'tp')
- new_max: float32 [1024, 8], P('kv', 'tp')
All inputs are finite; a program needn't handle non-finite values.
Results may differ from a plain program's by a relative error of at most 0.013.
Values may be sent and summed in bfloat16 or wider, within the bound.
A program may use at most 64 MiB of HBM per device.

v0:
```python
import jax
import jax.numpy as jnp
from jax import lax
from jax.sharding import PartitionSpec as P

D = 2048


def from_everyone(shard, axis):
    copies = jnp.broadcast_to(shard, (lax.axis_size(axis), *shard.shape))
    return lax.all_to_all(copies, axis, split_axis=0, concat_axis=0, tiled=True)


def in_order(blocks, dim):
    blocks = jnp.moveaxis(blocks, 0, dim)
    lengths = blocks.shape
    return blocks.reshape(*lengths[:dim], lengths[dim] * lengths[dim + 1], *lengths[dim + 2 :])


def collect(shard, axis, dim):
    blocks = from_everyone(shard, axis)
    return in_order(blocks, dim)


def of_everyone(shard, axis):
    return from_everyone(shard, axis).astype(jnp.float32).sum(axis=0)


def split_up(shard, dim, peers):
    before, after = (shard.shape[:dim], shard.shape[dim + 1 :])
    return jnp.moveaxis(shard.reshape(*before, peers, -1, *after), dim, 0)


def summed_on_arrival(shard, axis, dim):
    blocks = split_up(shard, dim, lax.axis_size(axis))
    arrived = lax.all_to_all(blocks, axis, split_axis=0, concat_axis=0, tiled=True)
    return arrived.astype(jnp.float32).sum(axis=0)


def activate(gate_sum, up_sum, square_sum):
    ffn_scale = lax.rsqrt(square_sum / D + 1e-06)[:, None]
    return (jax.nn.silu(ffn_scale * gate_sum) * (ffn_scale * up_sum)).astype(jnp.bfloat16)


def per_device(
    tokens,
    norm_gain,
    w_query,
    w_key,
    w_value,
    w_outgate,
    w_input_gate,
    w_forget_gate,
    memory,
    normalizer,
    memory_max,
    w_output,
    ffn_gain,
    w_gate,
    w_up,
    w_down,
):
    local_rows = tokens.shape[0]
    head_count = memory.shape[1]
    head_dim = memory.shape[2]
    full_rows = collect(tokens, "tp", 1)
    rows_f = full_rows.astype(jnp.float32)
    row_scale = lax.rsqrt(jnp.mean(rows_f * rows_f, axis=-1, keepdims=True) + 1e-06)
    normed = (rows_f * row_scale * norm_gain).astype(jnp.bfloat16)

    def project(weight):
        return jnp.dot(normed, weight, preferred_element_type=jnp.float32).reshape(
            local_rows, head_count, head_dim
        )

    queries = project(w_query) * head_dim ** (-0.5)
    key_vec = project(w_key)
    values = project(w_value)
    outgate = project(w_outgate)
    first_head = lax.axis_index("tp") * head_count
    igate = lax.dynamic_slice_in_dim(
        jnp.dot(normed, w_input_gate, preferred_element_type=jnp.float32), first_head, head_count, 1
    )
    forget_pre = lax.dynamic_slice_in_dim(
        jnp.dot(normed, w_forget_gate, preferred_element_type=jnp.float32),
        first_head,
        head_count,
        1,
    )
    lforget = jax.nn.log_sigmoid(forget_pre)
    new_max = jnp.maximum(lforget + memory_max, igate)
    keep_weight = jnp.exp(lforget + memory_max - new_max)
    admit_weight = jnp.exp(igate - new_max)
    new_memory = keep_weight[..., None, None] * memory + admit_weight[..., None, None] * (
        key_vec[..., :, None] * values[..., None, :]
    )
    new_normalizer = keep_weight[..., None] * normalizer + admit_weight[..., None] * key_vec
    numerator = jnp.einsum("bhd,bhdv->bhv", queries, new_memory, precision=lax.Precision.HIGHEST)
    denominator = jnp.sum(queries * new_normalizer, axis=-1)
    cell_out = numerator / jnp.maximum(jnp.abs(denominator), jnp.exp(-new_max))[..., None]
    head_mean = jnp.mean(cell_out, axis=-1, keepdims=True)
    centered = cell_out - head_mean
    head_var = jnp.mean(centered * centered, axis=-1, keepdims=True)
    mixed = (
        (jax.nn.sigmoid(outgate) * centered * lax.rsqrt(head_var + 1e-05))
        .reshape(local_rows, head_count * head_dim)
        .astype(jnp.bfloat16)
    )
    branch_out = jnp.dot(collect(mixed, "tp", 1), w_output, preferred_element_type=jnp.float32)
    resid = (tokens.astype(jnp.float32) + branch_out).astype(jnp.bfloat16)
    every_row = collect(resid, "kv", 0)
    every_f = every_row.astype(jnp.float32)
    square_part = jnp.sum(every_f * every_f, axis=-1)
    ffn_in = (every_f * ffn_gain).astype(jnp.bfloat16)
    gate_part = jnp.dot(ffn_in, w_gate, preferred_element_type=jnp.float32)
    up_part = jnp.dot(ffn_in, w_up, preferred_element_type=jnp.float32)
    gate_full, up_full, square_full = (
        of_everyone(gate_part.astype(jnp.bfloat16), "tp").astype(jnp.float32),
        of_everyone(up_part.astype(jnp.bfloat16), "tp").astype(jnp.float32),
        of_everyone(square_part.astype(jnp.bfloat16), "tp").astype(jnp.float32),
    )
    hidden = activate(gate_full, up_full, square_full)
    down_out = summed_on_arrival(
        jnp.dot(hidden, w_down, preferred_element_type=jnp.float32).astype(jnp.bfloat16), "kv", 0
    )
    result = (resid.astype(jnp.float32) + down_out).astype(jnp.bfloat16)
    return (result, new_memory, new_normalizer, new_max)


def solution(mesh):
    placed = (
        P("kv", "tp"),
        P(),
        P(None, "tp"),
        P(None, "tp"),
        P(None, "tp"),
        P(None, "tp"),
        P(),
        P(),
        P("kv", "tp", None, None),
        P("kv", "tp", None),
        P("kv", "tp"),
        P(None, "tp"),
        P("tp"),
        P("tp", "kv"),
        P("tp", "kv"),
        P("kv", "tp"),
    )
    return jax.shard_map(
        per_device,
        mesh=mesh,
        in_specs=placed,
        out_specs=(P("kv", "tp"), P("kv", "tp", None, None), P("kv", "tp", None), P("kv", "tp")),
        check_vma=False,
    )
```

profile of v0, /device:TPU:1, one launch (start us, length us, event | category | flops | bytes accessed | tf_op | source)
XLA Modules:
  0.0 148.2 jit_solution(9947505817167927230)
XLA Ops:
  0.6 0.0 copy-start
  0.7 1.4 broadcast_in_dim.12
  2.1 10.2 %all-to-all-start = ((bf16[8,16,256]{2,1,0:T(8,128)(2,1)}), bf16[8,16,256]{2,1,0:T(8,128)(2,1)S(1)}, u32[]{:S(2)}, u32[]{:S(2)}) async-start(bf16[8,16,256]{2,1,0:T(8,128)(2,1)} %broadcast_in_dim.12), calls=%async_computation | async-start | bytes 131072 | tf_op jit(solution)/shard_map/all_to_all | solution.py:11
  12.3 4.9 %all-to-all-done = bf16[8,16,256]{2,1,0:T(8,128)(2,1)S(1)} async-done(((bf16[8,16,256]{2,1,0:T(8,128)(2,1)}), bf16[8,16,256]{2,1,0:T(8,128)(2,1)S(1)}, u32[]{:S(2)}, u32[]{:S(2)}) %all-to-all-start) | async-done | bytes 65568 | tf_op jit(solution)/shard_map/all_to_all | solution.py:11
  17.2 0.1 fusion.12
  17.4 0.8 multiply_convert_fusion.2
  18.1 0.9 fusion.24
  19.0 0.9 fusion.23
  19.9 0.7 exponential_bitcast_fusion.1
  20.6 1.2 fusion.25
  21.9 0.2 fusion.26
  22.1 0.0 copy-done.13
  22.1 0.8 fusion.15
  22.9 0.0 copy-start.11
  22.9 0.4 multiply_add_fusion
  23.4 0.0 copy-start.1
  23.4 0.0 copy-start.4
  23.4 0.0 copy-start.8
  23.4 1.0 fusion.8
  24.4 0.2 fusion.21
  24.6 0.2 multiply_reduce_fusion.1
  24.8 0.2 fusion.6
  25.0 7.9 %all_to_all.36 = bf16[8,16,128]{2,1,0:T(8,128)(2,1)S(1)} all-to-all(bf16[8,16,128]{2,1,0:T(8,128)(2,1)S(1)} %broadcast_in_dim.13), channel_id=1, replica_groups=mesh['kv'=64,'tp'=8] {'tp'}, dimensions={0} | all-to-all | bytes 65536 | tf_op jit(solution)/shard_map/all_to_all | solution.py:11
  32.9 0.2 fusion
  33.1 0.0 copy-start.6
  33.1 29.2 %all_to_all.37 = bf16[64,16,256]{2,1,0:T(8,128)(2,1)S(1)} all-to-all(bf16[64,16,256]{2,1,0:T(8,128)(2,1)S(1)} %broadcast_in_dim.14), channel_id=1, replica_groups=mesh['kv'=64,'tp'=8] {'kv'}, dimensions={0} | all-to-all | bytes 1048576 | tf_op jit(solution)/shard_map/all_to_all | solution.py:11
  62.3 0.2 multiply_reduce_fusion
  62.5 0.1 convert_element_type.85
  62.6 0.5 broadcast.115
  63.2 0.7 reduce.9
  63.9 0.6 reshape.132
  64.5 6.4 %all-to-all-start.3 = ((bf16[8,2,512]{2,1,0:T(2,128)(2,1)}), bf16[8,2,512]{2,1,0:T(2,128)(2,1)S(1)}, u32[]{:S(2)}, u32[]{:S(2)}) async-start(bf16[8,2,512]{2,1,0:T(2,128)(2,1)} %reshape.132), calls=%async_computation.3 | async-start | bytes 32768 | tf_op jit(solution)/shard_map/all_to_all | solution.py:11
  70.9 0.1 fusion.7
  71.0 0.3 convolution_convert_fusion.2
  71.3 4.3 %all-to-all-done.3 = bf16[8,2,512]{2,1,0:T(2,128)(2,1)S(1)} async-done(((bf16[8,2,512]{2,1,0:T(2,128)(2,1)}), bf16[8,2,512]{2,1,0:T(2,128)(2,1)S(1)}, u32[]{:S(2)}, u32[]{:S(2)}) %all-to-all-start.3) | async-done | bytes 16416 | tf_op jit(solution)/shard_map/all_to_all | solution.py:11
  75.6 1.3 broadcast_in_dim.16
  76.9 4.3 %all-to-all-start.4 = ((bf16[8,1024,88]{1,2,0:T(8,128)(2,1)}), bf16[8,1024,88]{1,2,0:T(8,128)(2,1)S(1)}, u32[]{:S(2)}, u32[]{:S(2)}) async-start(bf16[8,1024,88]{1,2,0:T(8,128)(2,1)} %broadcast_in_dim.16), calls=%async_computation.4 | async-start | bytes 2883584 | tf_op jit(solution)/shard_map/all_to_all | solution.py:11
  81.2 0.3 convolution_convert_fusion.1
  81.5 18.9 %all-to-all-done.4 = bf16[8,1024,88]{1,2,0:T(8,128)(2,1)S(1)} async-done(((bf16[8,1024,88]{1,2,0:T(8,128)(2,1)}), bf16[8,1024,88]{1,2,0:T(8,128)(2,1)S(1)}, u32[]{:S(2)}, u32[]{:S(2)}) %all-to-all-start.4) | async-done | bytes 1441824 | tf_op jit(solution)/shard_map/all_to_all | solution.py:11
  100.4 1.3 broadcast_in_dim.34
  101.7 4.4 %all-to-all-start.5 = ((bf16[8,1024,88]{1,2,0:T(8,128)(2,1)}), bf16[8,1024,88]{1,2,0:T(8,128)(2,1)S(1)}, u32[]{:S(2)}, u32[]{:S(2)}) async-start(bf16[8,1024,88]{1,2,0:T(8,128)(2,1)} %broadcast_in_dim.34), calls=%async_computation.5 | async-start | bytes 2883584 | tf_op jit(solution)/shard_map/all_to_all | solution.py:11
  106.2 1.0 convert_reduce_fusion.1
  107.2 18.1 %all-to-all-done.5 = bf16[8,1024,88]{1,2,0:T(8,128)(2,1)S(1)} async-done(((bf16[8,1024,88]{1,2,0:T(8,128)(2,1)}), bf16[8,1024,88]{1,2,0:T(8,128)(2,1)S(1)}, u32[]{:S(2)}, u32[]{:S(2)}) %all-to-all-start.5) | async-done | bytes 1441824 | tf_op jit(solution)/shard_map/all_to_all | solution.py:11
  125.4 0.2 convert_reduce_fusion
  125.6 0.4 convolution_convert_fusion
  126.0 21.4 %all_to_all.38 = bf16[64,16,256]{2,1,0:T(8,128)(2,1)S(1)} all-to-all(bf16[64,16,256]{2,1,0:T(8,128)(2,1)S(1)} %bitcast.63), channel_id=1, replica_groups=mesh['kv'=64,'tp'=8] {'kv'}, dimensions={0} | all-to-all | bytes 1048576 | tf_op jit(solution)/shard_map/all_to_all | solution.py:36
  147.5 0.1 convert_reduce_fusion.2
  147.6 0.6 add_convert_fusion
  (34 shorter events, 0.2 us)
Async XLA Ops:
  0.6 21.4 %copy-start = (bf16[2048,128]{1,0:T(8,128)(2,1)S(1)}, bf16[2048,128]{1,0:T(8,128)(2,1)}, u32[]{:S(2)}) copy-start(bf16[2048,128]{1,0:T(8,128)(2,1)} %param.18) | copy-start | bytes 1572868
  0.6 21.2 %copy-start.3 = (bf16[2048,128]{1,0:T(8,128)(2,1)S(1)}, bf16[2048,128]{1,0:T(8,128)(2,1)}, u32[]{:S(2)}) copy-start(bf16[2048,128]{1,0:T(8,128)(2,1)} %param.20) | copy-start | bytes 1572868
  0.7 21.4 %copy-start.13 = (f32[16,1,128]{2,1,0:T(1,128)S(1)}, f32[16,1,128]{2,1,0:T(1,128)}, u32[]{:S(2)}) copy-start(f32[16,1,128]{2,1,0:T(1,128)} %param.25) | copy-start | bytes 24580
  2.1 20.8 %copy-start.2 = (f32[16,1,128,128]{3,2,1,0:T(8,128)S(1)}, f32[16,1,128,128]{3,2,1,0:T(8,128)}, u32[]{:S(2)}) copy-start(f32[16,1,128,128]{3,2,1,0:T(8,128)} %param.24) | copy-start | bytes 3145732
  2.1 15.1 %all-to-all-start = ((bf16[8,16,256]{2,1,0:T(8,128)(2,1)}), bf16[8,16,256]{2,1,0:T(8,128)(2,1)S(1)}, u32[]{:S(2)}, u32[]{:S(2)}) async-start(bf16[8,16,256]{2,1,0:T(8,128)(2,1)} %broadcast_in_dim.12), calls=%async_computation | async-start | bytes 131072 | tf_op jit(solution)/shard_map/all_to_all | solution.py:11
  20.6 2.7 %copy-start.9 = (f32[16,1]{0,1:T(1,128)}, f32[16,1]{0,1:T(1,128)S(1)}, u32[]{:S(2)}) copy-start(f32[16,1]{0,1:T(1,128)S(1)} %get-tuple-element.35) | copy-start | bytes 196
  22.9 1.8 %copy-start.11 = (bf16[2048,128]{1,0:T(8,128)(2,1)S(1)}, bf16[2048,128]{1,0:T(8,128)(2,1)}, u32[]{:S(2)}) copy-start(bf16[2048,128]{1,0:T(8,128)(2,1)} %param.21) | copy-start | bytes 1572868
  23.4 9.7 %copy-start.1 = (f32[16,1,128,128]{3,2,1,0:T(8,128)}, f32[16,1,128,128]{3,2,1,0:T(8,128)S(1)}, u32[]{:S(2)}) copy-start(f32[16,1,128,128]{3,2,1,0:T(8,128)S(1)} %multiply_add_fusion) | copy-start | bytes 3145732
  23.4 9.5 %copy-start.4 = (bf16[1024,256]{1,0:T(8,128)(2,1)S(1)}, bf16[1024,256]{1,0:T(8,128)(2,1)}, u32[]{:S(2)}) copy-start(bf16[1024,256]{1,0:T(8,128)(2,1)} %param.27) | copy-start | bytes 1572868
  23.4 9.5 %copy-start.8 = (bf16[16,256]{1,0:T(8,128)(2,1)S(1)}, bf16[16,256]{1,0:T(8,128)(2,1)}, u32[]{:S(2)}) copy-start(bf16[16,256]{1,0:T(8,128)(2,1)} %param.16) | copy-start | bytes 24580
  32.9 38.1 %copy-start.10 = (f32[256]{0:T(256)S(1)}, f32[256]{0:T(256)}, u32[]{:S(2)}) copy-start(f32[256]{0:T(256)} %param.28) | copy-start | bytes 3076
  33.1 37.9 %copy-start.6 = (bf16[256,88]{0,1:T(8,128)(2,1)S(1)}, bf16[256,88]{0,1:T(8,128)(2,1)}, u32[]{:S(2)}) copy-start(bf16[256,88]{0,1:T(8,128)(2,1)} %param.29) | copy-start | bytes 135172
  64.5 11.1 %all-to-all-start.3 = ((bf16[8,2,512]{2,1,0:T(2,128)(2,1)}), bf16[8,2,512]{2,1,0:T(2,128)(2,1)S(1)}, u32[]{:S(2)}, u32[]{:S(2)}) async-start(bf16[8,2,512]{2,1,0:T(2,128)(2,1)} %reshape.132), calls=%async_computation.3 | async-start | bytes 32768 | tf_op jit(solution)/shard_map/all_to_all | solution.py:11
  76.9 4.3 %copy-start.7 = (bf16[256,88]{0,1:T(8,128)(2,1)S(1)}, bf16[256,88]{0,1:T(8,128)(2,1)}, u32[]{:S(2)}) copy-start(bf16[256,88]{0,1:T(8,128)(2,1)} %param.30) | copy-start | bytes 135172
  76.9 23.5 %all-to-all-start.4 = ((bf16[8,1024,88]{1,2,0:T(8,128)(2,1)}), bf16[8,1024,88]{1,2,0:T(8,128)(2,1)S(1)}, u32[]{:S(2)}, u32[]{:S(2)}) async-start(bf16[8,1024,88]{1,2,0:T(8,128)(2,1)} %broadcast_in_dim.16), calls=%async_computation.4 | async-start | bytes 2883584 | tf_op jit(solution)/shard_map/all_to_all | solution.py:11
  101.7 23.7 %all-to-all-start.5 = ((bf16[8,1024,88]{1,2,0:T(8,128)(2,1)}), bf16[8,1024,88]{1,2,0:T(8,128)(2,1)S(1)}, u32[]{:S(2)}, u32[]{:S(2)}) async-start(bf16[8,1024,88]{1,2,0:T(8,128)(2,1)} %broadcast_in_dim.34), calls=%async_computation.5 | async-start | bytes 2883584 | tf_op jit(solution)/shard_map/all_to_all | solution.py:11
  106.2 19.4 %copy-start.12 = (bf16[88,256]{1,0:T(8,128)(2,1)S(1)}, bf16[88,256]{1,0:T(8,128)(2,1)}, u32[]{:S(2)}) copy-start(bf16[88,256]{1,0:T(8,128)(2,1)} %param.31) | copy-start | bytes 135172
  107.2 18.4 %copy-start.5 = (f32[1024,88]{0,1:T(8,128)S(1)}, f32[1024,88]{0,1:T(8,128)}, u32[]{:S(2)}) copy-start(f32[1024,88]{0,1:T(8,128)} %convert_reduce_fusion.1) | copy-start | bytes 1081348
where the time goes:
time: 151 us; the launch traced here: 148 us
  blocking collectives  58.5 us (39%)
  waiting for transfers between devices  46.2 us (31%)
  starting transfers between devices  25.4 us (17%)
  matrix products  6.35 us (4%)
  other arithmetic  5.44 us (4%)
  local copies, waits for them, and re-layouts  5.4 us (4%)
    all_to_all x4, waiting for transfers between devices, from_everyone(): return lax.all_to_all(copies, axis, split_axis=0, concat_axis=0, tiled=True)  46.2 us
    all_to_all x2, blocking collectives, from_everyone(): return lax.all_to_all(copies, axis, split_axis=0, concat_axis=0, tiled=True)  37 us
    all_to_all x4, starting transfers between devices, from_everyone(): return lax.all_to_all(copies, axis, split_axis=0, concat_axis=0, tiled=True)  25.4 us
    all_to_all x1, blocking collectives, summed_on_arrival(): lax.all_to_all(blocks, axis, split_axis=0, concat_axis=0, tiled=True)  21.4 us
    broadcast_in_dim x7, local copies, waits for them, and re-layouts, from_everyone(): copies = jnp.broadcast_to(shard, (lax.axis_size(axis), *shard.shape))  4.6 us
  transfers between devices with their start and end apart: 4, of which 4 were waited for; matrix products, arithmetic and copies ran while one was open for 1% of the time, Pallas kernels for 0%

commit v1 on v0

v1 whole, which is shorter than its diff:
```python
import functools

import jax
import jax.numpy as jnp
from jax import lax
from jax.experimental import pallas as pl
from jax.experimental.pallas import tpu as pltpu
from jax.sharding import PartitionSpec as P

EPS = 1e-06
HEAD_EPS = 1e-05
F32 = jnp.float32
BF16 = jnp.bfloat16
MESH = pl.DeviceIdType.MESH


def transposed_rhs(a, b):
    return lax.dot_general(a, b, (((1,), (1,)), ((), ())), preferred_element_type=F32)


def near_first(n):
    order = [0]
    for step in range(1, n // 2 + 1):
        order += [step] if step == n - step else [step, n - step]
    return order


def kernel(
    Z, Y, T, S, SHARD, PAD,
    tok_hbm, ngain_hbm, wq_hbm, wk_hbm, wv_hbm, wo_hbm, wig_hbm, wfg_hbm,
    mem_hbm, nrm_hbm, mmax_hbm, wout_hbm, fgain_hbm, wg_hbm, wu_hbm, wd_hbm,
    res_hbm, newmem_hbm, newnrm_hbm, newmax_hbm,
    tok, ngain, wproj, wgates, mem, nrm, mmax, wout, fgain, wgu, wd,
    newmem, newnrm, newmax, num, mixed, rows, csend, cbuf, hid, esend, ebuf, outv,
    load_sem, out_sem, a_send, a_recv, w_send, w_recv, m_send, m_recv, b_send, b_recv,
    c_send, c_recv, d_send, d_recv, e_send, e_recv,
):
    kv = lax.axis_index("kv")
    t = lax.axis_index("tp")
    z, y = kv // Y, kv % Y
    par = z % 2
    base = z - par
    R, CH = tok.shape[1], tok.shape[2]
    HD = mem.shape[1]
    width = T * CH
    GH = S * PAD

    def tp_peer(step):
        return (kv, (t + step) % T)

    def row_peer(dz, dy):
        return ((base + (par + dz) % 2) * Y + (y + dy) % Y, t)

    def weight_peer(step):
        return (((z + 2 * step) % Z) * Y + y, t)

    for s in range(S):
        for i in range(2):
            wgu[i, s, SHARD:PAD, :] = jnp.zeros((PAD - SHARD, CH), BF16)
        wd[s, SHARD:PAD, :] = jnp.zeros((PAD - SHARD, CH), BF16)
    loads = {}

    def load(name, src, dst):
        copy = pltpu.make_async_copy(src, dst, load_sem.at[len(loads)])
        copy.start()
        loads[name] = copy

    load("tok", tok_hbm, tok.at[t])
    load("wg", wg_hbm, wgu.at[0, 0, pl.ds(0, SHARD)])
    load("wu", wu_hbm, wgu.at[1, 0, pl.ds(0, SHARD)])
    load("wd", wd_hbm, wd.at[0, pl.ds(0, SHARD)])
    load("ngain", ngain_hbm, ngain)
    for i, w in enumerate((wq_hbm, wk_hbm, wv_hbm, wo_hbm)):
        load(f"w{i}", w, wproj.at[:, pl.ds(i * HD, HD)])
    load("wig", wig_hbm, wgates.at[0])
    load("wfg", wfg_hbm, wgates.at[1])
    load("mmax", mmax_hbm, mmax)
    load("nrm", nrm_hbm, nrm)
    load("mem", mem_hbm, mem)
    load("wout", wout_hbm, wout)
    load("fgain", fgain_hbm, fgain)

    barrier = pltpu.get_barrier_semaphore()
    peers = [tp_peer(step) for step in range(1, T)]
    peers += [row_peer(dz, dy) for dy in range(Y) for dz in range(2) if dz or dy]
    peers += [weight_peer(step) for step in range(1, S)]
    for peer in peers:
        pl.semaphore_signal(barrier, inc=1, device_id=peer, device_id_type=MESH)
    loads["tok"].wait()
    loads["wg"].wait()
    loads["wu"].wait()
    loads["wd"].wait()
    pl.semaphore_wait(barrier, len(peers))

    def send(src, dst, ssem, rsem, peer):
        copy = pltpu.make_async_remote_copy(
            src_ref=src, dst_ref=dst, send_sem=ssem, recv_sem=rsem,
            device_id=peer, device_id_type=MESH,
        )
        return copy

    a_copies = []
    for step in range(1, T):
        copy = send(tok.at[t], tok.at[t], a_send.at[step], a_recv.at[step], tp_peer(step))
        copy.start()
        a_copies.append(copy)
    w_copies = {}
    for i in range(3):
        for step in range(1, S):
            if i < 2:
                src, dst = wgu.at[i, 0, pl.ds(0, SHARD)], wgu.at[i, step, pl.ds(0, SHARD)]
            else:
                src, dst = wd.at[0, pl.ds(0, SHARD)], wd.at[step, pl.ds(0, SHARD)]
            copy = send(src, dst, w_send.at[i, step], w_recv.at[i, step], weight_peer(step))
            copy.start()
            w_copies[i, step] = copy

    for name in ("ngain", "w0", "w1", "w2", "w3", "wig", "wfg", "mmax", "nrm", "mem"):
        loads[name].wait()
    for copy in a_copies:
        copy.wait_recv()

    blocks = [tok[i].astype(F32) for i in range(T)]
    square = sum(jnp.sum(b * b, axis=-1, keepdims=True) for b in blocks)
    row_scale = lax.rsqrt(square / width + EPS)
    proj = jnp.zeros((R, 4 * HD), F32)
    ipre = jnp.zeros((R, wgates.shape[1]), F32)
    fpre = jnp.zeros((R, wgates.shape[1]), F32)
    for i in range(T):
        cols = slice(i * CH, (i + 1) * CH)
        normed = (blocks[i] * row_scale * ngain[:, cols]).astype(BF16)
        proj += jnp.dot(normed, wproj[cols, :], preferred_element_type=F32)
        ipre += transposed_rhs(normed, wgates[0, :, cols])
        fpre += transposed_rhs(normed, wgates[1, :, cols])
    queries = proj[:, :HD] * HD ** (-0.5)
    key_vec = proj[:, HD : 2 * HD]
    values = proj[:, 2 * HD : 3 * HD]
    outgate = proj[:, 3 * HD :]
    mine = lax.broadcasted_iota(jnp.int32, ipre.shape, 1) == t
    igate = jnp.sum(jnp.where(mine, ipre, 0.0), axis=-1, keepdims=True)
    fgate = jnp.sum(jnp.where(mine, fpre, 0.0), axis=-1, keepdims=True)
    lforget = jnp.minimum(fgate, 0.0) - jnp.log1p(jnp.exp(-jnp.abs(fgate)))
    eye = lax.broadcasted_iota(jnp.int32, (R, R), 0) == lax.broadcasted_iota(jnp.int32, (R, R), 1)
    old_max = jnp.sum(jnp.where(eye, jnp.broadcast_to(mmax[...], (R, R)), 0.0), axis=-1, keepdims=True)
    held = lforget + old_max
    new_max = jnp.maximum(held, igate)
    keep = jnp.exp(held - new_max)
    admit = jnp.exp(igate - new_max)

    new_normalizer = keep * nrm[:, 0, :] + admit * key_vec
    q_cols = queries.T
    for b in range(R):
        num[b : b + 1, :] = jnp.sum(mem[b] * q_cols[:, b : b + 1], axis=0, keepdims=True)
    q_k = jnp.sum(queries * key_vec, axis=-1, keepdims=True)
    numerator = keep * num[...] + (admit * q_k) * values
    denominator = jnp.sum(queries * new_normalizer, axis=-1, keepdims=True)
    cell_out = numerator / jnp.maximum(jnp.abs(denominator), jnp.exp(-new_max))
    centered = cell_out - jnp.mean(cell_out, axis=-1, keepdims=True)
    head_var = jnp.mean(centered * centered, axis=-1, keepdims=True)
    mixed[t] = (jax.nn.sigmoid(outgate) * centered * lax.rsqrt(head_var + HEAD_EPS)).astype(BF16)

    m_copies = []
    for step in range(1, T):
        copy = send(mixed.at[t], mixed.at[t], m_send.at[step], m_recv.at[step], tp_peer(step))
        copy.start()
        m_copies.append(copy)

    newnrm[:, 0, :] = new_normalizer
    newmax[...] = jnp.sum(jnp.where(eye, jnp.broadcast_to(new_max, (R, R)), 0.0), axis=0, keepdims=True)
    k_cols = (admit * key_vec).T
    for b in range(R):
        newmem[b] = keep[b : b + 1, :] * mem[b] + k_cols[:, b : b + 1] * values[b : b + 1, :]
    outs = [
        pltpu.make_async_copy(newmem, newmem_hbm, out_sem.at[0]),
        pltpu.make_async_copy(newnrm, newnrm_hbm, out_sem.at[1]),
        pltpu.make_async_copy(newmax, newmax_hbm, out_sem.at[2]),
    ]
    for copy in outs:
        copy.start()

    loads["wout"].wait()
    loads["fgain"].wait()
    for copy in m_copies:
        copy.wait_recv()
    branch = jnp.zeros((R, CH), F32)
    for i in range(0, T, 2):
        pair = jnp.concatenate([mixed[i], mixed[i + 1]], axis=-1)
        branch += jnp.dot(pair, wout[i * HD : (i + 2) * HD, :], preferred_element_type=F32)
    resid = (tok[t].astype(F32) + branch).astype(BF16)
    rows[0, 0] = resid

    b_copies = {}
    for dy in near_first(Y):
        for dz in range(2):
            if dz or dy:
                copy = send(rows.at[0, 0], rows.at[dy, dz], b_send.at[dy, dz], b_recv.at[dy, dz], row_peer(dz, dy))
                copy.start()
                b_copies[dy, dz] = copy

    for i in range(2):
        for step in range(1, S):
            w_copies[i, step].wait_recv()
    up_and_gate = wgu[...].reshape(2 * GH, CH)
    gain = fgain[...]
    lane = lax.broadcasted_iota(jnp.int32, (2 * R, 2 * GH), 1)

    c_copies = []
    for dy in near_first(Y):
        for dz in range(2):
            if dz or dy:
                b_copies[dy, dz].wait_recv()
        block = rows[dy].reshape(2 * R, CH).astype(F32)
        part = transposed_rhs((block * gain).astype(BF16), up_and_gate)
        square = jnp.sum(block * block, axis=-1, keepdims=True)
        high = square.astype(BF16).astype(F32)
        part = jnp.where(lane == SHARD, high, jnp.where(lane == SHARD + 1, square - high, part)).astype(BF16)
        owner = (y - dy + Y) % Y
        csend[dy] = part

        @pl.when(owner == t)
        def _():
            cbuf[t] = part

        step = (owner - t + T) % T
        copy = send(csend.at[dy], cbuf.at[t], c_send.at[dy], c_recv.at[step], (kv, owner))

        @pl.when(owner != t)
        def _():
            copy.start()

        c_copies.append((owner, copy))

    for step in range(1, T):
        send(csend.at[0], cbuf.at[(t - step + T) % T], c_send.at[0], c_recv.at[step], tp_peer(step)).wait_recv()
    total = cbuf[0].astype(F32)
    for i in range(1, T):
        total += cbuf[i].astype(F32)
    square = jnp.sum(jnp.where((lane == SHARD) | (lane == SHARD + 1), total, 0.0), axis=-1, keepdims=True)
    ffn_scale = lax.rsqrt(square / width + EPS)
    gate_act = ffn_scale * total[:, :GH]
    up_act = ffn_scale * total[:, GH:]
    hid[t] = (jax.nn.silu(gate_act) * up_act).astype(BF16)
    d_copies = []
    for step in range(1, T):
        copy = send(hid.at[t], hid.at[t], d_send.at[step], d_recv.at[step], tp_peer(step))
        copy.start()
        d_copies.append(copy)

    for step in range(1, S):
        w_copies[2, step].wait_recv()
    down = wd[...].reshape(GH, CH)
    e_copies = {}
    total = rows[0, 0].astype(F32)
    for dy in near_first(Y):
        owner = (y - dy + Y) % Y
        step = (t - owner + T) % T
        copy = send(hid.at[t], hid.at[owner], d_send.at[0], d_recv.at[step], (kv, owner))

        @pl.when(owner != t)
        def _():
            copy.wait_recv()

        part = jnp.dot(hid[owner], down, preferred_element_type=F32)
        if dy == 0:
            total += part[:R]
        esend[dy] = part.astype(BF16).reshape(2, R, CH)
        for dz in range(2):
            if dz or dy:
                copy = send(esend.at[dy, dz], ebuf.at[dy, dz], e_send.at[dy, dz], e_recv.at[dy, dz], row_peer(dz, Y - dy))
                copy.start()
                e_copies[dy, dz] = copy

    for dy in near_first(Y):
        for dz in range(2):
            if dz or dy:
                e_copies[dy, dz].wait_recv()
                total += ebuf[dy, dz].astype(F32)
    outv[...] = total.astype(BF16)
    out = pltpu.make_async_copy(outv, res_hbm, out_sem.at[3])
    out.start()

    for copy in [*a_copies, *w_copies.values(), *m_copies, *b_copies.values(), *d_copies, *e_copies.values()]:
        copy.wait_send()
    for owner, copy in c_copies:

        @pl.when(owner != t)
        def _():
            copy.wait_send()

    for copy in outs:
        copy.wait()
    out.wait()


def per_device(Z, Y, T, *args):
    (tokens, norm_gain, w_query, w_key, w_value, w_outgate, w_input_gate, w_forget_gate,
     memory, normalizer, memory_max, w_output, ffn_gain, w_gate, w_up, w_down) = args
    R, CH = tokens.shape
    width, HD = w_query.shape
    heads = w_input_gate.shape[1]
    inner = w_output.shape[0]
    SHARD = w_down.shape[0]
    S = Z // 2
    PAD = -(-(SHARD + 2) // 32) * 32
    GH = S * PAD
    any_spec = pl.BlockSpec(memory_space=pl.ANY)
    dma = pltpu.SemaphoreType.DMA
    outs = (
        jax.ShapeDtypeStruct((R, CH), BF16),
        jax.ShapeDtypeStruct((R, HD, HD), F32),
        jax.ShapeDtypeStruct((R, 1, HD), F32),
        jax.ShapeDtypeStruct((1, R), F32),
    )
    result, new_memory, new_normalizer, new_max = pl.pallas_call(
        functools.partial(kernel, Z, Y, T, S, SHARD, PAD),
        name="layer",
        out_shape=outs,
        in_specs=[any_spec] * 16,
        out_specs=(any_spec,) * 4,
        scratch_shapes=[
            pltpu.VMEM((T, R, CH), BF16),
            pltpu.VMEM((1, width), F32),
            pltpu.VMEM((width, 4 * HD), BF16),
            pltpu.VMEM((2, heads, width), BF16),
            pltpu.VMEM((R, HD, HD), F32),
            pltpu.VMEM((R, 1, HD), F32),
            pltpu.VMEM((1, R), F32),
            pltpu.VMEM((inner, CH), BF16),
            pltpu.VMEM((1, CH), F32),
            pltpu.VMEM((2, S, PAD, CH), BF16),
            pltpu.VMEM((S, PAD, CH), BF16),
            pltpu.VMEM((R, HD, HD), F32),
            pltpu.VMEM((R, 1, HD), F32),
            pltpu.VMEM((1, R), F32),
            pltpu.VMEM((R, HD), F32),
            pltpu.VMEM((T, R, HD), BF16),
            pltpu.VMEM((Y, 2, R, CH), BF16),
            pltpu.VMEM((Y, 2 * R, 2 * GH), BF16),
            pltpu.VMEM((T, 2 * R, 2 * GH), BF16),
            pltpu.VMEM((T, 2 * R, GH), BF16),
            pltpu.VMEM((Y, 2, R, CH), BF16),
            pltpu.VMEM((Y, 2, R, CH), BF16),
            pltpu.VMEM((R, CH), BF16),
            dma((16,)), dma((4,)), dma((T,)), dma((T,)), dma((3, S)), dma((3, S)), dma((T,)), dma((T,)),
            dma((Y, 2)), dma((Y, 2)), dma((Y,)), dma((T,)), dma((T,)), dma((T,)), dma((Y, 2)), dma((Y, 2)),
        ],
        compiler_params=pltpu.CompilerParams(collective_id=0, has_side_effects=True),
    )(
        tokens, norm_gain.reshape(1, width), w_query, w_key, w_value, w_outgate,
        w_input_gate.T, w_forget_gate.T, memory.reshape(R, HD, HD), normalizer, memory_max.T,
        w_output, ffn_gain.reshape(1, CH), w_gate.T, w_up.T, w_down,
    )
    return result, new_memory.reshape(R, 1, HD, HD), new_normalizer, new_max.T


def solution(mesh):
    placed = (
        P("kv", "tp"), P(),
        P(None, "tp"), P(None, "tp"), P(None, "tp"), P(None, "tp"),
        P(), P(),
        P("kv", "tp", None, None), P("kv", "tp", None), P("kv", "tp"),
        P(None, "tp"), P("tp"), P("tp", "kv"), P("tp", "kv"), P("kv", "tp"),
    )
    T = mesh.shape["tp"]
    Z, Y = mesh.shape["kv"] // T, T
    return jax.shard_map(
        functools.partial(per_device, Z, Y, T),
        mesh=mesh,
        in_specs=placed,
        out_specs=(P("kv", "tp"), P("kv", "tp", None, None), P("kv", "tp", None), P("kv", "tp")),
        check_vma=False,
    )
```

time: 151 us -> 55.7 us (0.37); the launches traced: 148 us -> 55.5 us
  blocking collectives: 58.5 us -> 0 us
  Pallas kernels: 0 us -> 50.1 us
  waiting for transfers between devices: 46.2 us -> 0 us
  starting transfers between devices: 25.4 us -> 0 us
  matrix products: 6.35 us -> 0 us
  other arithmetic: 5.44 us -> 0 us
    all_to_all x3 -> x0, blocking collectives: 58.5 us -> none  [the longest x2 37 us: from_everyone(): return lax.all_to_all(copies, axis, split_axis=0, concat_axis=0, tiled=True)]
    pallas_call x0 -> x1, Pallas kernels: none -> 50.1 us  [per_device(): pl.pallas_call(functools.partial(kernel, Z, Y, T, S, SHARD, PAD), name='l...]
    all_to_all x4 -> x0, waiting for transfers between devices: 46.2 us -> none  [from_everyone(): return lax.all_to_all(copies, axis, split_axis=0, concat_axis=0, tiled=True)]
    all_to_all x4 -> x0, starting transfers between devices: 25.4 us -> none  [from_everyone(): return lax.all_to_all(copies, axis, split_axis=0, concat_axis=0, tiled=True)]
    dot_general x11 -> x0, matrix products: 6.35 us -> none  [the longest x4 2.46 us: project(): jnp.dot(normed, weight, preferred_element_type=jnp.float32)]
    broadcast_in_dim x7 -> x0, local copies, waits for them, and re-layouts: 4.6 us -> none  [from_everyone(): copies = jnp.broadcast_to(shard, (lax.axis_size(axis), *shard.shape))]
    unnamed x30 -> x10, local copies, waits for them, and re-layouts: 0.7 us -> 4.77 us
    reduce_sum x8 -> x0, other arithmetic: 2.08 us -> none  [the longest x3 1.26 us: of_everyone(): return from_everyone(shard, axis).astype(jnp.float32).sum(axis=0)]
  transfers between devices with their start and end apart: 4 -> 0, of which waited for: 4 -> 0; matrix products, arithmetic and copies ran while one was open for 1% -> 0% of each run, Pallas kernels for 0% -> 0%
where the time goes in v1:
time: 55.7 us; the launch traced here: 55.5 us
  Pallas kernels  50.1 us (90%)
  local copies, waits for them, and re-layouts  4.77 us (9%)
  between operations  0.66 us (1%)
    pallas_call x1, Pallas kernels, per_device(): pl.pallas_call(functools.partial(kernel, Z, Y, T, S, SHARD, PAD), name='l...  50.1 us
    unnamed x10, local copies, waits for them, and re-layouts  4.77 us

profile of v1, /device:TPU:1, one launch (start us, length us, event | category | flops | bytes accessed | tf_op | source)
XLA Modules:
  0.0 55.5 jit_solution(199073013329146564)
XLA Ops:
  0.6 50.1 %layer.1 = (bf16[16,256]{1,0:T(8,128)(2,1)}, f32[16,128,128]{2,1,0:T(8,128)}, f32[16,1,128]{2,1,0:T(1,128)}, f32[1,16]{1,0:T(1,128)}) custom-call(bf16[16,256]{1,0:T(8,128)(2,1)} %tok_hbm.1, f32[1,2048]{1,0:T(1,128)} %bitcast.18, bf16[2048,128]{1,0:T(8,128)(2,1)} %wq_hbm.1, bf16[2048,128]{1,0:T(8,128)(2,1)} %wk_hbm.1, bf16[2048,128]{1,0:T(8,128)(2,1)} %wv_hbm.1, ...), custom_call_target="tpu_custom_call" | custom-call | tf_op jit(solution)/shard_map/layer/pallas_call | solution.py:314
  50.7 0.0 copy-start.1
  50.7 0.7 %copy-done.1 = bf16[16,256]{1,0:T(8,128)(2,1)S(1)} copy-done((bf16[16,256]{1,0:T(8,128)(2,1)S(1)}, bf16[16,256]{1,0:T(8,128)(2,1)}, u32[]{:S(2)}) %copy-start.1) | copy-done | bytes 8216
  51.4 0.6 %copy.25 = bf16[16,256]{1,0:T(8,128)(2,1)} copy(bf16[16,256]{1,0:T(8,128)(2,1)S(1)} %copy-done.1) | data formatting | bytes 16384
  52.0 0.0 copy-start
  52.0 2.3 %copy.26 = f32[16,1,128,128]{3,2,1,0:T(8,128)} copy(f32[16,1,128,128]{3,2,1,0:T(8,128)} %bitcast.12) | data formatting | bytes 2097152
  54.3 0.0 copy-done
  54.3 0.0 copy-start.2
  54.3 0.6 %copy.27 = f32[16,1,128]{2,1,0:T(1,128)} copy(f32[16,1,128]{2,1,0:T(1,128)S(1)} %copy-done) | data formatting | bytes 16384
  54.9 0.1 copy-done.2
  55.0 0.5 copy.28
Async XLA Ops:
  50.7 0.7 %copy-start.1 = (bf16[16,256]{1,0:T(8,128)(2,1)S(1)}, bf16[16,256]{1,0:T(8,128)(2,1)}, u32[]{:S(2)}) copy-start(bf16[16,256]{1,0:T(8,128)(2,1)} %get-tuple-element.20) | copy-start | bytes 24580
  52.0 2.3 %copy-start = (f32[16,1,128]{2,1,0:T(1,128)S(1)}, f32[16,1,128]{2,1,0:T(1,128)}, u32[]{:S(2)}) copy-start(f32[16,1,128]{2,1,0:T(1,128)} %get-tuple-element.22) | copy-start | bytes 24580
  54.3 0.7 %copy-start.2 = (f32[1,16]{1,0:T(1,128)S(1)}, f32[1,16]{1,0:T(1,128)}, u32[]{:S(2)}) copy-start(f32[1,16]{1,0:T(1,128)} %get-tuple-element.11) | copy-start | bytes 196

commit v2 on v1

--- a/solution.py
+++ b/solution.py
@@ -29,10 +29,10 @@
     Z, Y, T, S, SHARD, PAD,
     tok_hbm, ngain_hbm, wq_hbm, wk_hbm, wv_hbm, wo_hbm, wig_hbm, wfg_hbm,
     mem_hbm, nrm_hbm, mmax_hbm, wout_hbm, fgain_hbm, wg_hbm, wu_hbm, wd_hbm,
-    res_hbm, newmem_hbm, newnrm_hbm, newmax_hbm,
-    tok, ngain, wproj, wgates, mem, nrm, mmax, wout, fgain, wgu, wd,
-    newmem, newnrm, newmax, num, mixed, rows, csend, cbuf, hid, esend, ebuf, outv,
-    load_sem, out_sem, a_send, a_recv, w_send, w_recv, m_send, m_recv, b_send, b_recv,
+    outv, newmem, newnrm, newmax,
+    tok, ngain, wproj, wgates, mem, nrm, mmax, wout, fgain, mix,
+    num, mixed, rows, csend, cbuf, hid, esend, ebuf,
+    load_sem, up_sem, ready, a_send, a_recv, w_send, w_recv, m_send, m_recv, b_send, b_recv,
     c_send, c_recv, d_send, d_recv, e_send, e_recv,
 ):
     kv = lax.axis_index("kv")
@@ -51,13 +51,12 @@
     def row_peer(dz, dy):
         return ((base + (par + dz) % 2) * Y + (y + dy) % Y, t)
 
-    def weight_peer(step):
-        return (((z + 2 * step) % Z) * Y + y, t)
+    def column(other):
+        return (other * Y + y, t)
 
     for s in range(S):
-        for i in range(2):
-            wgu[i, s, SHARD:PAD, :] = jnp.zeros((PAD - SHARD, CH), BF16)
-        wd[s, SHARD:PAD, :] = jnp.zeros((PAD - SHARD, CH), BF16)
+        for i in range(3):
+            mix[i, s, SHARD:PAD, :] = jnp.zeros((PAD - SHARD, CH), BF16)
     loads = {}
 
     def load(name, src, dst):
@@ -66,9 +65,9 @@
         loads[name] = copy
 
     load("tok", tok_hbm, tok.at[t])
-    load("wg", wg_hbm, wgu.at[0, 0, pl.ds(0, SHARD)])
-    load("wu", wu_hbm, wgu.at[1, 0, pl.ds(0, SHARD)])
-    load("wd", wd_hbm, wd.at[0, pl.ds(0, SHARD)])
+    load("wg", wg_hbm, mix.at[0, 0, pl.ds(0, SHARD)])
+    load("wu", wu_hbm, mix.at[1, 0, pl.ds(0, SHARD)])
+    load("wd", wd_hbm, mix.at[2, 0, pl.ds(0, SHARD)])
     load("ngain", ngain_hbm, ngain)
     for i, w in enumerate((wq_hbm, wk_hbm, wv_hbm, wo_hbm)):
         load(f"w{i}", w, wproj.at[:, pl.ds(i * HD, HD)])
@@ -82,15 +81,25 @@
 
     barrier = pltpu.get_barrier_semaphore()
     peers = [tp_peer(step) for step in range(1, T)]
-    peers += [row_peer(dz, dy) for dy in range(Y) for dz in range(2) if dz or dy]
-    peers += [weight_peer(step) for step in range(1, S)]
+    peers += [row_peer(dz, dy) for dy in near_first(Y) for dz in range(2) if dz or dy]
     for peer in peers:
         pl.semaphore_signal(barrier, inc=1, device_id=peer, device_id_type=MESH)
+    beside = z - 1 + 2 * par
+    inner = (beside >= 0) & (beside < Z)
+
+    @pl.when(inner)
+    def _():
+        pl.semaphore_signal(barrier, inc=1, device_id=column(beside), device_id_type=MESH)
+
     loads["tok"].wait()
-    loads["wg"].wait()
-    loads["wu"].wait()
-    loads["wd"].wait()
-    pl.semaphore_wait(barrier, len(peers))
+
+    @pl.when(inner)
+    def _():
+        pl.semaphore_wait(barrier, len(peers) + 1)
+
+    @pl.when(jnp.logical_not(inner))
+    def _():
+        pl.semaphore_wait(barrier, len(peers))
 
     def send(src, dst, ssem, rsem, peer):
         copy = pltpu.make_async_remote_copy(
@@ -104,16 +113,58 @@
         copy = send(tok.at[t], tok.at[t], a_send.at[step], a_recv.at[step], tp_peer(step))
         copy.start()
         a_copies.append(copy)
-    w_copies = {}
-    for i in range(3):
+
+    @pl.when(z > 0)
+    def _():
+        pl.semaphore_wait(up_sem, 1)
+
+    @pl.when(z < Z - 1)
+    def _():
+        pl.semaphore_signal(up_sem, inc=1, device_id=column(z + 1), device_id_type=MESH)
+
+    for step in range(1, S):
+
+        @pl.when(z >= 2 * step)
+        def _():
+            pl.semaphore_signal(ready.at[step], inc=1, device_id=column(z - 2 * step), device_id_type=MESH)
+
+    def shard_copy(piece, above, step):
+        part = pl.ds(0, 2) if piece == 0 else pl.ds(2, 1)
+        slot = S - step if above else step
+        other = z + 2 * step if above else z - 2 * step
+        return send(
+            mix.at[part, 0, pl.ds(0, SHARD)], mix.at[part, slot, pl.ds(0, SHARD)],
+            w_send.at[piece, above, step], w_recv.at[piece, slot], column(other),
+        )
+
+    def shard_exists(above, step):
+        return z + 2 * step < Z if above else z >= 2 * step
+
+    def to_below(piece):
         for step in range(1, S):
-            if i < 2:
-                src, dst = wgu.at[i, 0, pl.ds(0, SHARD)], wgu.at[i, step, pl.ds(0, SHARD)]
-            else:
-                src, dst = wd.at[0, pl.ds(0, SHARD)], wd.at[step, pl.ds(0, SHARD)]
-            copy = send(src, dst, w_send.at[i, step], w_recv.at[i, step], weight_peer(step))
-            copy.start()
-            w_copies[i, step] = copy
+
+            @pl.when(shard_exists(0, step))
+            def _():
+                shard_copy(piece, 0, step).start()
+
+    def to_above(steps):
+        for step in steps:
+
+            @pl.when(shard_exists(1, step))
+            def _():
+                pl.semaphore_wait(ready.at[step], 1)
+                shard_copy(0, 1, step).start()
+                shard_copy(1, 1, step).start()
+
+    def shard_arrives(piece):
+        for slot in range(1, S):
+            shard_copy(piece, 0, slot).wait_recv()
+
+    loads["wg"].wait()
+    loads["wu"].wait()
+    loads["wd"].wait()
+    to_below(0)
+    to_below(1)
 
     for name in ("ngain", "w0", "w1", "w2", "w3", "wig", "wfg", "mmax", "nrm", "mem"):
         loads[name].wait()
@@ -165,18 +216,12 @@
         copy.start()
         m_copies.append(copy)
 
+    to_above(range(1, 2))
     newnrm[:, 0, :] = new_normalizer
     newmax[...] = jnp.sum(jnp.where(eye, jnp.broadcast_to(new_max, (R, R)), 0.0), axis=0, keepdims=True)
     k_cols = (admit * key_vec).T
     for b in range(R):
         newmem[b] = keep[b : b + 1, :] * mem[b] + k_cols[:, b : b + 1] * values[b : b + 1, :]
-    outs = [
-        pltpu.make_async_copy(newmem, newmem_hbm, out_sem.at[0]),
-        pltpu.make_async_copy(newnrm, newnrm_hbm, out_sem.at[1]),
-        pltpu.make_async_copy(newmax, newmax_hbm, out_sem.at[2]),
-    ]
-    for copy in outs:
-        copy.start()
 
     loads["wout"].wait()
     loads["fgain"].wait()
@@ -197,10 +242,9 @@
                 copy.start()
                 b_copies[dy, dz] = copy
 
-    for i in range(2):
-        for step in range(1, S):
-            w_copies[i, step].wait_recv()
-    up_and_gate = wgu[...].reshape(2 * GH, CH)
+    to_above(range(2, S))
+    shard_arrives(0)
+    up_and_gate = mix[0:2].reshape(2 * GH, CH)
     gain = fgain[...]
     lane = lax.broadcasted_iota(jnp.int32, (2 * R, 2 * GH), 1)
 
@@ -246,9 +290,8 @@
         copy.start()
         d_copies.append(copy)
 
-    for step in range(1, S):
-        w_copies[2, step].wait_recv()
-    down = wd[...].reshape(GH, CH)
+    shard_arrives(1)
+    down = mix[2].reshape(GH, CH)
     e_copies = {}
     total = rows[0, 0].astype(F32)
     for dy in near_first(Y):
@@ -276,10 +319,7 @@
                 e_copies[dy, dz].wait_recv()
                 total += ebuf[dy, dz].astype(F32)
     outv[...] = total.astype(BF16)
-    out = pltpu.make_async_copy(outv, res_hbm, out_sem.at[3])
-    out.start()
-
-    for copy in [*a_copies, *w_copies.values(), *m_copies, *b_copies.values(), *d_copies, *e_copies.values()]:
+    for copy in [*a_copies, *m_copies, *b_copies.values(), *d_copies, *e_copies.values()]:
         copy.wait_send()
     for owner, copy in c_copies:
 
@@ -287,9 +327,22 @@
         def _():
             copy.wait_send()
 
-    for copy in outs:
+    for above in range(2):
+        for step in range(1, S):
+
+            @pl.when(shard_exists(above, step))
+            def _():
+                shard_copy(0, above, step).wait_send()
+                shard_copy(1, above, step).wait_send()
+
+
+def store(*refs):
+    sem = refs[-1]
+    copies = [pltpu.make_async_copy(refs[i], refs[4 + i], sem.at[i]) for i in range(4)]
+    for copy in copies:
+        copy.start()
+    for copy in copies:
         copy.wait()
-    out.wait()
 
 
 def per_device(Z, Y, T, *args):
@@ -311,12 +364,12 @@
         jax.ShapeDtypeStruct((R, 1, HD), F32),
         jax.ShapeDtypeStruct((1, R), F32),
     )
-    result, new_memory, new_normalizer, new_max = pl.pallas_call(
+    held = pl.pallas_call(
         functools.partial(kernel, Z, Y, T, S, SHARD, PAD),
         name="layer",
-        out_shape=outs,
+        out_shape=tuple(pltpu.VMEM(o.shape, o.dtype) for o in outs),
         in_specs=[any_spec] * 16,
-        out_specs=(any_spec,) * 4,
+        out_specs=(pl.BlockSpec(memory_space=pltpu.VMEM),) * 4,
         scratch_shapes=[
             pltpu.VMEM((T, R, CH), BF16),
             pltpu.VMEM((1, width), F32),
@@ -327,11 +380,7 @@
             pltpu.VMEM((1, R), F32),
             pltpu.VMEM((inner, CH), BF16),
             pltpu.VMEM((1, CH), F32),
-            pltpu.VMEM((2, S, PAD, CH), BF16),
-            pltpu.VMEM((S, PAD, CH), BF16),
-            pltpu.VMEM((R, HD, HD), F32),
-            pltpu.VMEM((R, 1, HD), F32),
-            pltpu.VMEM((1, R), F32),
+            pltpu.VMEM((3, S, PAD, CH), BF16),
             pltpu.VMEM((R, HD), F32),
             pltpu.VMEM((T, R, HD), BF16),
             pltpu.VMEM((Y, 2, R, CH), BF16),
@@ -340,8 +389,8 @@
             pltpu.VMEM((T, 2 * R, GH), BF16),
             pltpu.VMEM((Y, 2, R, CH), BF16),
             pltpu.VMEM((Y, 2, R, CH), BF16),
-            pltpu.VMEM((R, CH), BF16),
-            dma((16,)), dma((4,)), dma((T,)), dma((T,)), dma((3, S)), dma((3, S)), dma((T,)), dma((T,)),
+            dma((16,)), pltpu.SemaphoreType.REGULAR, pltpu.SemaphoreType.REGULAR((S,)),
+            dma((T,)), dma((T,)), dma((2, 2, S)), dma((2, S)), dma((T,)), dma((T,)),
             dma((Y, 2)), dma((Y, 2)), dma((Y,)), dma((T,)), dma((T,)), dma((T,)), dma((Y, 2)), dma((Y, 2)),
         ],
         compiler_params=pltpu.CompilerParams(collective_id=0, has_side_effects=True),
@@ -350,6 +399,14 @@
         w_input_gate.T, w_forget_gate.T, memory.reshape(R, HD, HD), normalizer, memory_max.T,
         w_output, ffn_gain.reshape(1, CH), w_gate.T, w_up.T, w_down,
     )
+    result, new_memory, new_normalizer, new_max = pl.pallas_call(
+        store,
+        name="store",
+        out_shape=outs,
+        in_specs=[pl.BlockSpec(memory_space=pltpu.VMEM)] * 4,
+        out_specs=(any_spec,) * 4,
+        scratch_shapes=[dma((4,))],
+    )(*[pltpu.with_memory_space_constraint(h, pltpu.VMEM) for h in held])
     return result, new_memory.reshape(R, 1, HD, HD), new_normalizer, new_max.T
 
 

time: 55.7 us -> 47.9 us (0.86)
  local copies, waits for them, and re-layouts: 4.77 us -> 0 us
  Pallas kernels: 50.1 us -> 47.1 us
    unnamed x10 -> x0, local copies, waits for them, and re-layouts: 4.77 us -> none
    pallas_call x1, Pallas kernels: 50.1 us -> 46.1 us  [per_device(): pl.pallas_call(functools.partial(kernel, Z, Y, T, S, SHARD, PAD), name='l...]
    pallas_call x0 -> x1, Pallas kernels: none -> 1.02 us  [per_device(): pl.pallas_call(store, name='store', out_shape=outs, in_specs=[pl.BlockSpe...]
where the time goes in v2:
time: 47.9 us; the launch traced here: 47.7 us
  Pallas kernels  47.1 us (98%)
  between operations  0.65 us (1%)
    pallas_call x1, Pallas kernels, per_device(): pl.pallas_call(functools.partial(kernel, Z, Y, T, S, SHARD, PAD), name='l...  46.1 us
    pallas_call x1, Pallas kernels, per_device(): pl.pallas_call(store, name='store', out_shape=outs, in_specs=[pl.BlockSpe...  1.02 us

profile of v2, /device:TPU:1, one launch (start us, length us, event | category | flops | bytes accessed | tf_op | source)
XLA Modules:
  0.0 47.7 jit_solution(154721473486862628)
XLA Ops:
  0.6 46.1 %layer.1 = (bf16[16,256]{1,0:T(8,128)(2,1)S(1)}, f32[16,128,128]{2,1,0:T(8,128)S(1)}, f32[16,1,128]{2,1,0:T(1,128)S(1)}, f32[1,16]{1,0:T(1,128)S(1)}) custom-call(bf16[16,256]{1,0:T(8,128)(2,1)} %tok_hbm.1, f32[1,2048]{1,0:T(1,128)} %bitcast.17, bf16[2048,128]{1,0:T(8,128)(2,1)} %wq_hbm.1, bf16[2048,128]{1,0:T(8,128)(2,1)} %wk_hbm.1, ...), custom_call_target="tpu_custom_call" | custom-call | tf_op jit(solution)/shard_map/layer/pallas_call | solution.py:367
  46.7 1.0 %store.1 = (bf16[16,256]{1,0:T(8,128)(2,1)}, f32[16,128,128]{2,1,0:T(8,128)}, f32[16,1,128]{2,1,0:T(1,128)}, f32[1,16]{1,0:T(1,128)}) custom-call(bf16[16,256]{1,0:T(8,128)(2,1)S(1)} %get-tuple-element.12.refs_0_, f32[16,128,128]{2,1,0:T(8,128)S(1)} %get-tuple-element.13.refs_1_, f32[16,1,128]{2,1,0:T(1,128)S(1)} %get-tuple-element.14.refs_2_, ...), custom_call_target="tpu_custom_call" | custom-call | tf_op jit(solution)/shard_map/store/pallas_call | solution.py:402

commit v3 on v2

v3 whole, which is shorter than its diff:
```python
import functools

import jax
import jax.numpy as jnp
from jax import lax
from jax.experimental import pallas as pl
from jax.experimental.pallas import tpu as pltpu
from jax.sharding import PartitionSpec as P

EPS = 1e-06
HEAD_EPS = 1e-05
F32 = jnp.float32
BF16 = jnp.bfloat16
MESH = pl.DeviceIdType.MESH


def transposed_rhs(a, b):
    return lax.dot_general(a, b, (((1,), (1,)), ((), ())), preferred_element_type=F32)


def near_first(n):
    order = [0]
    for step in range(1, n // 2 + 1):
        order += [step] if step == n - step else [step, n - step]
    return order


def kernel(
    Z, Y, T, S, SHARD, PAD,
    tok_hbm, ngain_hbm, wq_hbm, wk_hbm, wv_hbm, wo_hbm, wig_hbm, wfg_hbm,
    mem_hbm, nrm_hbm, mmax_hbm, wout_hbm, fgain_hbm, wg_hbm, wu_hbm, wd_hbm,
    outv, newmem, newnrm, newmax,
    tok, ngain, wproj, wgates, mem, nrm, mmax, wout, fgain, mix,
    num, mixed, resid_buf, rows, csend, cbuf, hid, esend, ebuf,
    load_sem, up_sem, ready, a_send, a_recv, w_send, w_recv, r_send, r_recv, p_send, p_recv, g_send, g_recv,
    m_send, m_recv, b_send, b_recv, c_send, c_recv, d_send, d_recv, e_send, e_recv,
):
    kv = lax.axis_index("kv")
    t = lax.axis_index("tp")
    z, y = kv // Y, kv % Y
    x, core = t // 2, t % 2
    par = z % 2
    base = z - par
    R, CH = tok.shape[1], tok.shape[2]
    HD = mem.shape[1]
    X, K = T // 2, Y // 2
    width = T * CH
    GH = S * PAD
    odd = (y + core) % 2
    home = y % 2
    at_home = core == home
    middle = (z >= 2) & (z < Z - 2)
    order = [k // 2 if k % 2 == 0 else K - 1 - k // 2 for k in range(K)]

    def tp_peer(step):
        return (kv, (t + step) % T)

    def row_peer(dz, dy, side):
        return ((base + (par + dz) % 2) * Y + (y + dy) % Y, 2 * x + side)

    def column(other):
        return (other * Y + y, t)

    above, below = (z + 2) % Z, (z + Z - 2) % Z
    partner = (kv, 2 * x + 1 - core)

    def send(src, dst, ssem, rsem, peer):
        return pltpu.make_async_remote_copy(
            src_ref=src, dst_ref=dst, send_sem=ssem, recv_sem=rsem,
            device_id=peer, device_id_type=MESH,
        )

    loads = {}

    def load(name, src, dst):
        copy = pltpu.make_async_copy(src, dst, load_sem.at[len(loads)])
        copy.start()
        loads[name] = copy

    for side in range(2):
        for s in range(S):
            for i in range(3):
                mix[side, i, s, SHARD:PAD, :] = jnp.zeros((PAD - SHARD, CH), BF16)
    load("tok", tok_hbm, tok.at[t])
    load("wg", wg_hbm, mix.at[core, 0, 0, pl.ds(0, SHARD)])
    load("wu", wu_hbm, mix.at[core, 1, 0, pl.ds(0, SHARD)])
    load("wd", wd_hbm, mix.at[core, 2, 0, pl.ds(0, SHARD)])
    load("ngain", ngain_hbm, ngain)
    for i, w in enumerate((wq_hbm, wk_hbm, wv_hbm, wo_hbm)):
        load(f"w{i}", w, wproj.at[:, pl.ds(i * HD, HD)])
    load("wig", wig_hbm, wgates.at[0])
    load("wfg", wfg_hbm, wgates.at[1])
    load("mmax", mmax_hbm, mmax)
    load("nrm", nrm_hbm, nrm)
    load("mem", mem_hbm, mem)
    load("wout", wout_hbm, wout)
    load("fgain", fgain_hbm, fgain.at[core])

    barrier = pltpu.get_barrier_semaphore()
    peers = [tp_peer(step) for step in range(1, T)]
    for dy in near_first(Y):
        for dz in range(2):
            if dz or dy:
                peers += [row_peer(dz, dy, 0), row_peer(dz, dy, 1)]
    for peer in peers:
        pl.semaphore_signal(barrier, inc=1, device_id=peer, device_id_type=MESH)
    beside = z - 1 + 2 * par
    inner = (beside >= 0) & (beside < Z)

    @pl.when(inner)
    def _():
        pl.semaphore_signal(barrier, inc=1, device_id=column(beside), device_id_type=MESH)

    loads["tok"].wait()

    @pl.when(inner)
    def _():
        pl.semaphore_wait(barrier, len(peers) + 1)

    @pl.when(jnp.logical_not(inner))
    def _():
        pl.semaphore_wait(barrier, len(peers))

    a_copies = []
    for step in range(1, T):
        copy = send(tok.at[t], tok.at[t], a_send.at[step], a_recv.at[step], tp_peer(step))
        copy.start()
        a_copies.append(copy)

    @pl.when(z > 0)
    def _():
        pl.semaphore_wait(up_sem, 1)

    @pl.when(z < Z - 1)
    def _():
        pl.semaphore_signal(up_sem, inc=1, device_id=column(z + 1), device_id_type=MESH)

    @pl.when(z >= 2)
    def _():
        pl.semaphore_signal(ready.at[0], inc=1, device_id=column(below), device_id_type=MESH)

    @pl.when(z >= Z - 2)
    def _():
        pl.semaphore_signal(ready.at[1], inc=1, device_id=column(above), device_id_type=MESH)

    def piece_at(piece, slot):
        part = pl.ds(0, 2) if piece == 0 else pl.ds(2, 1)
        return mix.at[core, part, slot, pl.ds(0, SHARD)]

    def direct(piece, up):
        slot = S - 1 if up else 1
        return send(piece_at(piece, 0), piece_at(piece, slot), w_send.at[piece, up], w_recv.at[piece, slot],
                    column(above if up else below))

    def relay(piece, up):
        return send(piece_at(piece, S - 1 if up else 1), piece_at(piece, 2), r_send.at[piece, up], r_recv.at[piece],
                    column(above if up else below))

    def forward(piece, slot):
        return send(piece_at(piece, slot), piece_at(piece, slot), p_send.at[piece, slot], p_recv.at[piece, slot], partner)

    def direct_both(up):
        direct(0, up).start()
        direct(1, up).start()

    def pass_on(piece, relayed):
        for up in range(2):
            slot = S - 1 if up else 1
            direct(piece, 1 if slot == S - 1 else 0).wait_recv()
            if relayed:
                relay(piece, up).start()
            forward(piece, slot).start()

    loads["wg"].wait()
    loads["wu"].wait()
    loads["wd"].wait()

    @pl.when(z >= 2)
    def _():
        direct_both(0)

    @pl.when(z >= Z - 2)
    def _():
        direct_both(1)

    forward(0, 0).start()
    forward(1, 0).start()
    loads["fgain"].wait()
    gain_copy = send(fgain.at[core], fgain.at[core], g_send, g_recv, partner)
    gain_copy.start()

    for name in ("ngain", "w0", "w1", "w2", "w3", "wig", "wfg", "mmax", "nrm", "mem"):
        loads[name].wait()
    for copy in a_copies:
        copy.wait_recv()

    @pl.when(z < Z - 2)
    def _():
        pl.semaphore_wait(ready.at[0], 1)
        direct_both(1)

    blocks = [tok[i].astype(F32) for i in range(T)]
    square = sum(jnp.sum(b * b, axis=-1, keepdims=True) for b in blocks)
    row_scale = lax.rsqrt(square / width + EPS)
    proj = jnp.zeros((R, 4 * HD), F32)
    ipre = jnp.zeros((R, wgates.shape[1]), F32)
    fpre = jnp.zeros((R, wgates.shape[1]), F32)
    for i in range(T):
        cols = slice(i * CH, (i + 1) * CH)
        normed = (blocks[i] * row_scale * ngain[:, cols]).astype(BF16)
        proj += jnp.dot(normed, wproj[cols, :], preferred_element_type=F32)
        ipre += transposed_rhs(normed, wgates[0, :, cols])
        fpre += transposed_rhs(normed, wgates[1, :, cols])
    queries = proj[:, :HD] * HD ** (-0.5)
    key_vec = proj[:, HD : 2 * HD]
    values = proj[:, 2 * HD : 3 * HD]
    outgate = proj[:, 3 * HD :]
    mine = lax.broadcasted_iota(jnp.int32, ipre.shape, 1) == t
    igate = jnp.sum(jnp.where(mine, ipre, 0.0), axis=-1, keepdims=True)
    fgate = jnp.sum(jnp.where(mine, fpre, 0.0), axis=-1, keepdims=True)
    lforget = jnp.minimum(fgate, 0.0) - jnp.log1p(jnp.exp(-jnp.abs(fgate)))
    eye = lax.broadcasted_iota(jnp.int32, (R, R), 0) == lax.broadcasted_iota(jnp.int32, (R, R), 1)
    old_max = jnp.sum(jnp.where(eye, jnp.broadcast_to(mmax[...], (R, R)), 0.0), axis=-1, keepdims=True)
    held = lforget + old_max
    new_max = jnp.maximum(held, igate)
    keep = jnp.exp(held - new_max)
    admit = jnp.exp(igate - new_max)

    new_normalizer = keep * nrm[:, 0, :] + admit * key_vec
    q_cols = queries.T
    for b in range(R):
        num[b : b + 1, :] = jnp.sum(mem[b] * q_cols[:, b : b + 1], axis=0, keepdims=True)
    q_k = jnp.sum(queries * key_vec, axis=-1, keepdims=True)
    numerator = keep * num[...] + (admit * q_k) * values
    denominator = jnp.sum(queries * new_normalizer, axis=-1, keepdims=True)
    cell_out = numerator / jnp.maximum(jnp.abs(denominator), jnp.exp(-new_max))
    centered = cell_out - jnp.mean(cell_out, axis=-1, keepdims=True)
    head_var = jnp.mean(centered * centered, axis=-1, keepdims=True)
    mixed[t] = (jax.nn.sigmoid(outgate) * centered * lax.rsqrt(head_var + HEAD_EPS)).astype(BF16)

    m_copies = []
    for step in range(1, T):
        copy = send(mixed.at[t], mixed.at[t], m_send.at[step], m_recv.at[step], tp_peer(step))
        copy.start()
        m_copies.append(copy)

    newnrm[:, 0, :] = new_normalizer
    newmax[...] = jnp.sum(jnp.where(eye, jnp.broadcast_to(new_max, (R, R)), 0.0), axis=0, keepdims=True)
    k_cols = (admit * key_vec).T
    for b in range(R):
        newmem[b] = keep[b : b + 1, :] * mem[b] + k_cols[:, b : b + 1] * values[b : b + 1, :]

    @pl.when(middle)
    def _():
        pass_on(0, True)

    loads["wout"].wait()
    for copy in m_copies:
        copy.wait_recv()
    branch = jnp.zeros((R, CH), F32)
    for i in range(0, T, 2):
        pair = jnp.concatenate([mixed[i], mixed[i + 1]], axis=-1)
        branch += jnp.dot(pair, wout[i * HD : (i + 2) * HD, :], preferred_element_type=F32)
    resid = (tok[t].astype(F32) + branch).astype(BF16)
    resid_buf[...] = resid

    def row_copy(dy, dz):
        return send(resid_buf, rows.at[dy // 2, core, dz], b_send.at[dy, dz], b_recv.at[dy // 2, core, dz],
                    row_peer(dz, dy, home))

    for dy in near_first(Y):
        for dz in range(2):
            if dz or dy:
                row_copy(dy, dz).start()

    @pl.when(at_home)
    def _():
        rows[0, core, 0] = resid

    @pl.when(jnp.logical_not(at_home))
    def _():
        row_copy(0, 0).start()

    @pl.when(z < 2)
    def _():
        pl.semaphore_wait(ready.at[1], 1)
        direct_both(0)

    @pl.when(jnp.logical_not(middle))
    def _():
        pass_on(0, False)

    relay(0, 0).wait_recv()
    forward(0, 2).start()

    @pl.when(middle)
    def _():
        pass_on(1, True)

    @pl.when(jnp.logical_not(middle))
    def _():
        pass_on(1, False)

    for slot in range(S):
        forward(0, slot).wait_recv()

    up_and_gate = [mix[side, 0:2].reshape(2 * GH, CH) for side in range(2)]
    gain_copy.wait_recv()
    gain = [fgain[side] for side in range(2)]
    lane = lax.broadcasted_iota(jnp.int32, (2 * R, 2 * GH), 1)
    c_copies = []
    group = max(1, K // 2)
    for first in range(0, K, group):
        ks = order[first : first + group]
        for k in ks:
            for side in range(2):
                for dz in range(2):
                    copy = send(resid_buf, rows.at[k, side, dz], b_send.at[0, 0], b_recv.at[k, side, dz], partner)
                    if k or dz:
                        copy.wait_recv()
                    else:

                        @pl.when(jnp.logical_not(at_home & (core == side)))
                        def _():
                            copy.wait_recv()

        total = 0.0
        square = 0.0
        for side in range(2):
            block = jnp.concatenate([rows[k, side].reshape(2 * R, CH) for k in ks], axis=0).astype(F32)
            square += jnp.sum(block * block, axis=-1, keepdims=True)
            total += transposed_rhs((block * gain[side]).astype(BF16), up_and_gate[side])
        for i, k in enumerate(ks):
            part = total[i * 2 * R : (i + 1) * 2 * R]
            sq = square[i * 2 * R : (i + 1) * 2 * R]
            high = sq.astype(BF16).astype(F32)
            part = jnp.where(lane == SHARD, high, jnp.where(lane == SHARD + 1, sq - high, part)).astype(BF16)
            owner = (y - 2 * k - odd + 2 * Y) % Y
            csend[k] = part

            @pl.when(owner == t)
            def _():
                cbuf[x] = part

            copy = send(csend.at[k], cbuf.at[x], c_send.at[k], c_recv.at[x], (kv, owner))

            @pl.when(owner != t)
            def _():
                copy.start()

            c_copies.append((owner, copy))

    for step in range(1, X):
        sender = (x + step) % X
        send(csend.at[0], cbuf.at[sender], c_send.at[0], c_recv.at[sender], (kv, 2 * sender + core)).wait_recv()
    total = cbuf[0].astype(F32)
    for i in range(1, X):
        total += cbuf[i].astype(F32)
    square = jnp.sum(jnp.where((lane == SHARD) | (lane == SHARD + 1), total, 0.0), axis=-1, keepdims=True)
    ffn_scale = lax.rsqrt(square / width + EPS)
    gate_act = ffn_scale * total[:, :GH]
    up_act = ffn_scale * total[:, GH:]
    hid[x] = (jax.nn.silu(gate_act) * up_act).astype(BF16)
    d_copies = []
    for step in range(1, X):
        copy = send(hid.at[x], hid.at[x], d_send.at[step], d_recv.at[x], (kv, 2 * ((x + step) % X) + core))
        copy.start()
        d_copies.append(copy)

    relay(1, 0).wait_recv()
    forward(1, 2).start()
    for slot in range(S):
        forward(1, slot).wait_recv()
    down = [mix[side, 2].reshape(GH, CH) for side in range(2)]
    e_copies = []
    for k in order:
        owner = (y - 2 * k - odd + 2 * Y) % Y
        source = owner // 2
        copy = send(hid.at[source], hid.at[source], d_send.at[0], d_recv.at[source], (kv, owner))

        @pl.when(source != x)
        def _():
            copy.wait_recv()

        own = hid[source]
        for side in range(2):
            part = jnp.dot(own, down[side], preferred_element_type=F32).astype(BF16)
            esend[k, side] = part.reshape(2, R, CH)
            for dz in range(2):
                dy = 2 * k + odd
                copy = send(esend.at[k, side, dz], ebuf.at[dy, dz], e_send.at[k, side, dz], e_recv.at[dy, dz],
                            row_peer(dz, 2 * Y - dy, side))
                away = jnp.logical_not((odd == 0) & (core == side)) if k == 0 and dz == 0 else None
                e_copies.append((away, copy))
                if away is None:
                    copy.start()
                else:
                    pl.when(away)(copy.start)

                    @pl.when(jnp.logical_not(away))
                    def _():
                        ebuf[0, 0] = part[:R]

    total = resid.astype(F32)
    for dy in near_first(Y):
        for dz in range(2):
            copy = send(esend.at[0, 0, dz], ebuf.at[dy, dz], e_send.at[0, 0, dz], e_recv.at[dy, dz], partner)
            if dz or dy:
                copy.wait_recv()
            else:
                pl.when(jnp.logical_not(at_home))(copy.wait_recv)
    for dy in range(Y):
        for dz in range(2):
            total += ebuf[dy, dz].astype(F32)
    outv[...] = total.astype(BF16)

    for copy in [*a_copies, *m_copies, *d_copies, gain_copy]:
        copy.wait_send()
    for dy in range(Y):
        for dz in range(2):
            if dz or dy:
                row_copy(dy, dz).wait_send()
    pl.when(jnp.logical_not(at_home))(row_copy(0, 0).wait_send)
    for owner, copy in c_copies:
        pl.when(owner != t)(copy.wait_send)
    for away, copy in e_copies:
        if away is None:
            copy.wait_send()
        else:
            pl.when(away)(copy.wait_send)
    for piece in range(2):
        for up in range(2):
            direct(piece, up).wait_send()
            pl.when(middle)(relay(piece, up).wait_send)
        for slot in range(S):
            forward(piece, slot).wait_send()


def store(*refs):
    sem = refs[-1]
    copies = [pltpu.make_async_copy(refs[i], refs[4 + i], sem.at[i]) for i in range(4)]
    for copy in copies:
        copy.start()
    for copy in copies:
        copy.wait()


def per_device(Z, Y, T, *args):
    (tokens, norm_gain, w_query, w_key, w_value, w_outgate, w_input_gate, w_forget_gate,
     memory, normalizer, memory_max, w_output, ffn_gain, w_gate, w_up, w_down) = args
    R, CH = tokens.shape
    width, HD = w_query.shape
    heads = w_input_gate.shape[1]
    inner = w_output.shape[0]
    SHARD = w_down.shape[0]
    S = Z // 2
    PAD = -(-(SHARD + 2) // 32) * 32
    GH = S * PAD
    any_spec = pl.BlockSpec(memory_space=pl.ANY)
    dma = pltpu.SemaphoreType.DMA
    outs = (
        jax.ShapeDtypeStruct((R, CH), BF16),
        jax.ShapeDtypeStruct((R, HD, HD), F32),
        jax.ShapeDtypeStruct((R, 1, HD), F32),
        jax.ShapeDtypeStruct((1, R), F32),
    )
    held = pl.pallas_call(
        functools.partial(kernel, Z, Y, T, S, SHARD, PAD),
        name="layer",
        out_shape=tuple(pltpu.VMEM(o.shape, o.dtype) for o in outs),
        in_specs=[any_spec] * 16,
        out_specs=(pl.BlockSpec(memory_space=pltpu.VMEM),) * 4,
        scratch_shapes=[
            pltpu.VMEM((T, R, CH), BF16),
            pltpu.VMEM((1, width), F32),
            pltpu.VMEM((width, 4 * HD), BF16),
            pltpu.VMEM((2, heads, width), BF16),
            pltpu.VMEM((R, HD, HD), F32),
            pltpu.VMEM((R, 1, HD), F32),
            pltpu.VMEM((1, R), F32),
            pltpu.VMEM((inner, CH), BF16),
            pltpu.VMEM((2, 1, CH), F32),
            pltpu.VMEM((2, 3, S, PAD, CH), BF16),
            pltpu.VMEM((R, HD), F32),
            pltpu.VMEM((T, R, HD), BF16),
            pltpu.VMEM((R, CH), BF16),
            pltpu.VMEM((Y // 2, 2, 2, R, CH), BF16),
            pltpu.VMEM((Y // 2, 2 * R, 2 * GH), BF16),
            pltpu.VMEM((T // 2, 2 * R, 2 * GH), BF16),
            pltpu.VMEM((T // 2, 2 * R, GH), BF16),
            pltpu.VMEM((Y // 2, 2, 2, R, CH), BF16),
            pltpu.VMEM((Y, 2, R, CH), BF16),
            dma((16,)), pltpu.SemaphoreType.REGULAR, pltpu.SemaphoreType.REGULAR((2,)),
            dma((T,)), dma((T,)), dma((2, 2)), dma((2, S)), dma((2, 2)), dma((2,)), dma((2, S)), dma((2, S)), dma, dma,
            dma((T,)), dma((T,)), dma((Y, 2)), dma((Y // 2, 2, 2)), dma((Y // 2,)), dma((T // 2,)),
            dma((T // 2,)), dma((T // 2,)), dma((Y // 2, 2, 2)), dma((Y, 2)),
        ],
        compiler_params=pltpu.CompilerParams(collective_id=0, has_side_effects=True),
    )(
        tokens, norm_gain.reshape(1, width), w_query, w_key, w_value, w_outgate,
        w_input_gate.T, w_forget_gate.T, memory.reshape(R, HD, HD), normalizer, memory_max.T,
        w_output, ffn_gain.reshape(1, CH), w_gate.T, w_up.T, w_down,
    )
    result, new_memory, new_normalizer, new_max = pl.pallas_call(
        store,
        name="store",
        out_shape=outs,
        in_specs=[pl.BlockSpec(memory_space=pltpu.VMEM)] * 4,
        out_specs=(any_spec,) * 4,
        scratch_shapes=[dma((4,))],
    )(*[pltpu.with_memory_space_constraint(h, pltpu.VMEM) for h in held])
    return result, new_memory.reshape(R, 1, HD, HD), new_normalizer, new_max.T


def solution(mesh):
    placed = (
        P("kv", "tp"), P(),
        P(None, "tp"), P(None, "tp"), P(None, "tp"), P(None, "tp"),
        P(), P(),
        P("kv", "tp", None, None), P("kv", "tp", None), P("kv", "tp"),
        P(None, "tp"), P("tp"), P("tp", "kv"), P("tp", "kv"), P("kv", "tp"),
    )
    T = mesh.shape["tp"]
    Z, Y = mesh.shape["kv"] // T, T
    return jax.shard_map(
        functools.partial(per_device, Z, Y, T),
        mesh=mesh,
        in_specs=placed,
        out_specs=(P("kv", "tp"), P("kv", "tp", None, None), P("kv", "tp", None), P("kv", "tp")),
        check_vma=False,
    )
```

time: 47.9 us -> 45.4 us (0.948)
  Pallas kernels: 47.1 us -> 44.6 us
    pallas_call x1, Pallas kernels: 46.1 us -> 43.6 us  [per_device(): pl.pallas_call(functools.partial(kernel, Z, Y, T, S, SHARD, PAD), name='l...]
where the time goes in v3:
time: 45.4 us; the launch traced here: 45.3 us
  Pallas kernels  44.6 us (98%)
  between operations  0.65 us (1%)
    pallas_call x1, Pallas kernels, per_device(): pl.pallas_call(functools.partial(kernel, Z, Y, T, S, SHARD, PAD), name='l...  43.6 us
    pallas_call x1, Pallas kernels, per_device(): pl.pallas_call(store, name='store', out_shape=outs, in_specs=[pl.BlockSpe...  1.02 us

profile of v3, /device:TPU:1, one launch (start us, length us, event | category | flops | bytes accessed | tf_op | source)
XLA Modules:
  0.0 45.3 jit_solution(4055610618720538974)
XLA Ops:
  0.6 43.6 %layer.1 = (bf16[16,256]{1,0:T(8,128)(2,1)S(1)}, f32[16,128,128]{2,1,0:T(8,128)S(1)}, f32[16,1,128]{2,1,0:T(1,128)S(1)}, f32[1,16]{1,0:T(1,128)S(1)}) custom-call(bf16[16,256]{1,0:T(8,128)(2,1)} %tok_hbm.1, f32[1,2048]{1,0:T(1,128)} %bitcast.17, bf16[2048,128]{1,0:T(8,128)(2,1)} %wq_hbm.1, bf16[2048,128]{1,0:T(8,128)(2,1)} %wk_hbm.1, ...), custom_call_target="tpu_custom_call" | custom-call | tf_op jit(solution)/shard_map/layer/pallas_call | solution.py:467
  44.2 1.0 %store.1 = (bf16[16,256]{1,0:T(8,128)(2,1)}, f32[16,128,128]{2,1,0:T(8,128)}, f32[16,1,128]{2,1,0:T(1,128)}, f32[1,16]{1,0:T(1,128)}) custom-call(bf16[16,256]{1,0:T(8,128)(2,1)S(1)} %get-tuple-element.12.refs_0_, f32[16,128,128]{2,1,0:T(8,128)S(1)} %get-tuple-element.13.refs_1_, f32[16,1,128]{2,1,0:T(1,128)S(1)} %get-tuple-element.14.refs_2_, ...), custom_call_target="tpu_custom_call" | custom-call | tf_op jit(solution)/shard_map/store/pallas_call | solution.py:504
